TPU v7x, 32 devices: a whole 2x2x4 slice. The times are simulated.
32 devices in a mesh: sp: 8 (over z, x), tp: 4 (over y, core).
Axes of the slice: x: 2, y: 2, z: 4, core: 2. Of those that a mesh axis runs over, the one named last changes fastest.
Arguments:
- tokens: bfloat16 [4096, 2048], P('sp', 'tp'), may hold values from -400 to 400
- lru_in: bfloat16 [2048, 1024], P(None, 'tp'), may hold values from -0.125 to 0.125
- lru_gate_in: bfloat16 [2048, 1024], P(None, 'tp'), may hold values from -0.125 to 0.125
- query_w: bfloat16 [2048, 1024], P(None, 'tp'), may hold values from -1 to 1
- key_w: bfloat16 [2048, 1024], P(None, 'tp'), may hold values from -10 to 10
- value_w: bfloat16 [2048, 1024], P(None, 'tp'), may hold values from -0.125 to 0.125
- conv_weight: bfloat16 [4, 1024], replicated, may hold values from -3 to 3
- recur_gate_w: bfloat16 [16, 64, 64], replicated, may hold values from -0.75 to 0.75
- input_gate_w: bfloat16 [16, 64, 64], replicated, may hold values from -0.75 to 0.75
- rate_param: float32 [1024], replicated, may hold values from 0 to 16
- decay_extra: float32 [4096, 1024], P('sp', 'tp'), may hold values from -2 to 0
- forget_cum: float32 [4096, 8], P('sp', 'tp'), may hold values from -386 to 0, as said below
- out_lru: bfloat16 [1024, 2048], P('tp'), may hold values from -0.1875 to 0.1875
- out_fox: bfloat16 [1024, 2048], P('tp'), may hold values from -0.1875 to 0.1875
Outputs:
- mixed_out: bfloat16 [4096, 2048], P('sp', 'tp')
Inputs may be any that keep to these rules, and one draw needn't show every extreme that they name: `forget_cum`: non-increasing along positions in every head.
All inputs are finite; a program needn't handle non-finite values.
Results may differ from a plain program's by a relative error of at most 0.014.
Values may be sent and summed in bfloat16 or wider, within the bound.
A program may use at most 64 MiB of HBM per device.

v0:
```python
import math

import jax
import jax.numpy as jnp
from jax import lax
from jax.sharding import PartitionSpec as P

D = 2048
HEAD_DIM = 128


decay_sharpness = 8.0
epsilon_norm = 1e-06


def from_behind(block, axis, distance):
    devices = range(lax.axis_size(axis))
    route = [(i - distance, i) for i in devices if i - distance in devices]
    return lax.ppermute(block, axis, route)


def entering(part, axis, combine, identity):
    place = lax.axis_index(axis)
    gathered = jax.tree.map(lambda a: lax.all_gather(a, axis), part)
    state = jax.tree.map(lambda a, e: jnp.zeros_like(a) + jnp.asarray(e, a.dtype), part, identity)

    def one(hop, state):
        return combine(
            state, jax.tree.map(lambda a: lax.dynamic_index_in_dim(a, hop, 0, False), gathered)
        )

    return lax.fori_loop(0, place, one, state)


def combine_pairs(earlier, later):
    decay_one, state_one = earlier
    decay_two, state_two = later
    return (decay_one * decay_two, decay_two * state_one + state_two)


def shards(
    tokens,
    lru_in,
    lru_gate_in,
    query_w,
    key_w,
    value_w,
    conv_weight,
    recur_gate_w,
    input_gate_w,
    rate_param,
    decay_extra,
    forget_cum,
    out_lru,
    out_fox,
):
    tok_rows = tokens.shape[0]
    lru_cols = lru_in.shape[1]
    fox_cols = query_w.shape[1]
    tp_index = lax.axis_index("tp")
    weight_all = jnp.concatenate([lru_in, lru_gate_in, query_w, key_w, value_w], 1)
    portion = lax.all_gather(tokens, "tp", axis=1, tiled=True)
    weight_part = weight_all
    portion_f32 = portion.astype(jnp.float32)
    projected = jnp.dot(portion, weight_part, preferred_element_type=jnp.float32)
    squares = jnp.sum(portion_f32 * portion_f32, axis=1)
    row_scale = lax.rsqrt(squares / D + epsilon_norm)
    scaled = (projected * row_scale[:, None]).astype(jnp.bfloat16)
    lru_input = scaled[:, :lru_cols]
    gate_input = scaled[:, lru_cols : 2 * lru_cols]
    queries = scaled[:, 2 * lru_cols : 2 * lru_cols + fox_cols]
    keys_dev = scaled[:, 2 * lru_cols + fox_cols : 2 * lru_cols + 2 * fox_cols]
    values_dev = scaled[:, 2 * lru_cols + 2 * fox_cols :]
    taps = conv_weight.shape[0]
    own_conv = lax.dynamic_slice_in_dim(conv_weight, tp_index * lru_cols, lru_cols, 1)
    earlier_rows = from_behind(lru_input[tok_rows - (taps - 1) :], "sp", 1)
    padded = jnp.concatenate([earlier_rows, lru_input], 0)
    conv_sum = jnp.zeros((tok_rows, lru_cols), jnp.float32)
    for tap_idx in range(taps):
        conv_sum = conv_sum + own_conv[tap_idx].astype(jnp.float32)[None, :] * padded[
            tap_idx : tap_idx + tok_rows
        ].astype(jnp.float32)
    conv_out = conv_sum.astype(jnp.bfloat16)
    block_width = recur_gate_w.shape[1]
    blocks_dev = lru_cols // block_width
    own_recur = lax.dynamic_slice_in_dim(recur_gate_w, tp_index * blocks_dev, blocks_dev, 0)
    own_input = lax.dynamic_slice_in_dim(input_gate_w, tp_index * blocks_dev, blocks_dev, 0)
    blocked = conv_out.reshape(tok_rows, blocks_dev, block_width)
    recur_gate = jax.nn.sigmoid(
        jnp.einsum("tnc,ncd->tnd", blocked, own_recur, preferred_element_type=jnp.float32).reshape(
            tok_rows, lru_cols
        )
    )
    input_gate = jax.nn.sigmoid(
        jnp.einsum("tnc,ncd->tnd", blocked, own_input, preferred_element_type=jnp.float32).reshape(
            tok_rows, lru_cols
        )
    )
    own_rate = lax.dynamic_slice_in_dim(rate_param, tp_index * lru_cols, lru_cols, 0)
    log_decay = -decay_sharpness * jax.nn.softplus(-own_rate)[None, :] * recur_gate + decay_extra
    driven = jnp.sqrt(-jnp.expm1(2.0 * log_decay)) * input_gate * conv_out.astype(jnp.float32)
    prefix, local_states = lax.associative_scan(combine_pairs, (jnp.exp(log_decay), driven), axis=0)
    identity = (jnp.ones((lru_cols,), jnp.float32), jnp.zeros((lru_cols,), jnp.float32))
    incoming = entering(
        (prefix[tok_rows - 1], local_states[tok_rows - 1]), "sp", combine_pairs, identity
    )
    states = local_states + prefix * incoming[1][None, :]
    lru_out = (states * jax.nn.gelu(gate_input.astype(jnp.float32))).astype(jnp.bfloat16)
    heads_dev = fox_cols // HEAD_DIM
    score_scale = HEAD_DIM ** (-0.5)
    gates_all = lax.all_gather(forget_cum, "sp", axis=0, tiled=True)
    sp_index = lax.axis_index("sp")
    offset = sp_index * tok_rows
    query_sets = (queries, offset)
    groups = []
    query_rows, query_first = query_sets
    count = query_rows.shape[0]
    query_heads = query_rows.reshape(count, heads_dev, HEAD_DIM)
    query_cum = lax.dynamic_slice_in_dim(gates_all, query_first, count, 0).T
    query_pos = query_first + jnp.arange(count)
    groups.append((query_heads, query_cum, query_pos, query_first + count - 1))

    def key_block(running, group, key_rows, value_rows, key_first):
        query_heads, query_cum, query_pos, last_query = group
        length = key_rows.shape[0]

        def active(current):
            maxima, totals, weighted = current
            key_cum = lax.dynamic_slice_in_dim(gates_all, key_first, length, 0).T
            key_heads = key_rows.reshape(length, heads_dev, HEAD_DIM)
            value_heads = value_rows.reshape(length, heads_dev, HEAD_DIM)
            scores = (
                jnp.einsum(
                    "qhd,khd->hqk", query_heads, key_heads, preferred_element_type=jnp.float32
                )
                * score_scale
            )
            scores = scores + query_cum[:, :, None] - key_cum[:, None, :]
            key_pos = key_first + jnp.arange(length)
            causal = (query_pos[:, None] >= key_pos[None, :])[None]
            scores = jnp.where(causal, scores, -1e30)
            new_maxima = jnp.maximum(maxima, jnp.max(scores, axis=2))
            probs = jnp.where(causal, jnp.exp(scores - new_maxima[:, :, None]), 0.0)
            rescale = jnp.exp(maxima - new_maxima)
            new_totals = totals * rescale + jnp.sum(probs, axis=2)
            new_weighted = weighted * rescale[:, :, None] + jnp.einsum(
                "hqk,khd->hqd",
                probs.astype(jnp.bfloat16),
                value_heads,
                preferred_element_type=jnp.float32,
            )
            return (new_maxima, new_totals, new_weighted)

        def unchanged(current):
            return current

        return lax.cond(key_first <= last_query, active, unchanged, running)

    def visit_all(running, key_rows, value_rows, key_first):
        return tuple(
            (
                key_block(running[slot], groups[slot], key_rows, value_rows, key_first)
                for slot in range(len(groups))
            )
        )

    attn_start = tuple(
        (
            (
                jnp.full((heads_dev, group[0].shape[0]), -1e30, jnp.float32),
                jnp.zeros((heads_dev, group[0].shape[0]), jnp.float32),
                jnp.zeros((heads_dev, group[0].shape[0], HEAD_DIM), jnp.float32),
            )
            for group in groups
        )
    )
    key_rows = lax.all_gather(keys_dev, "sp", axis=0, tiled=True)
    value_rows = lax.all_gather(values_dev, "sp", axis=0, tiled=True)
    length = key_rows.shape[0]
    blk_len = math.gcd(length, 1024)
    block_count = length // blk_len
    key_blocks = key_rows.reshape(block_count, blk_len, key_rows.shape[1])
    value_blocks = value_rows.reshape(block_count, blk_len, value_rows.shape[1])

    def visit_block(current, block_item):
        block_keys, block_values, block_number = block_item
        return (visit_all(current, block_keys, block_values, block_number * blk_len), None)

    result, unused_out = lax.scan(
        visit_block, attn_start, (key_blocks, value_blocks, jnp.arange(block_count))
    )
    results = []
    for maxima, totals, weighted in result:
        count = weighted.shape[1]
        results.append(
            (weighted / totals[:, :, None])
            .transpose(1, 0, 2)
            .reshape(count, fox_cols)
            .astype(jnp.bfloat16)
        )
    fox_out = results[0]
    branch = jnp.concatenate([lru_out, fox_out], 1)
    weight_rows = jnp.concatenate([out_lru, out_fox], 0)
    weight_part = weight_rows
    mixed_out = lax.psum_scatter(
        lax.dot_general(
            weight_part, branch, (((0,), (1,)), ((), ())), preferred_element_type=jnp.float32
        ).astype(jnp.bfloat16),
        "tp",
        scatter_dimension=0,
        tiled=True,
    ).astype(jnp.float32)
    return mixed_out.T.astype(jnp.bfloat16)


def solution(mesh):
    placed = (
        P("sp", "tp"),
        P(None, "tp"),
        P(None, "tp"),
        P(None, "tp"),
        P(None, "tp"),
        P(None, "tp"),
        P(),
        P(),
        P(),
        P(),
        P("sp", "tp"),
        P("sp", "tp"),
        P("tp", None),
        P("tp", None),
    )
    return jax.shard_map(
        shards, mesh=mesh, in_specs=placed, out_specs=P("sp", "tp"), check_vma=False
    )
```

profile of v0, /device:TPU:25, one launch (start us, length us, event | category | flops | bytes accessed | tf_op | source)
XLA Modules:
  0.0 220.9 jit_solution(8571016639987610162)
XLA Ops:
  7.3 2.4 %constant_dynamic-update-slice_fusion.4 = bf16[2048,1280]{1,0:T(8,128)(2,1)} fusion(bf16[2048,256]{1,0:T(8,128)(2,1)} %param.21), kind=kLoop, calls=%fused_computation.103 | loop fusion | bytes 2097152
  9.8 2.4 %constant_dynamic-update-slice_fusion.3 = bf16[2048,1280]{1,0:T(8,128)(2,1)} fusion(bf16[2048,1280]{1,0:T(8,128)(2,1)} %constant_dynamic-update-slice_fusion.4, bf16[2048,256]{1,0:T(8,128)(2,1)} %param.22), kind=kLoop, calls=%fused_computation.102 | loop fusion | bytes 2097152
  15.5 17.3 %all-gather.6.cloned.1.call-done = bf16[512,2048]{1,0:T(8,128)(2,1)} async-done(((bf16[512,512]{1,0:T(8,128)(2,1)}), bf16[512,2048]{1,0:T(8,128)(2,1)}) %all-gather.6.cloned.1.call-update) | async-done | bytes 2097168 | tf_op jit(solution)/shard_map/all_gather | solution.py:62
  32.9 2.1 multiply_reduce_fusion
  35.0 6.0 %fusion.15 = bf16[512,1280]{1,0:T(8,128)(2,1)S(1)} fusion(bf16[512,2048]{1,0:T(8,128)(2,1)} %all-gather.6.cloned.1.call-done, bf16[2048,1280]{1,0:T(8,128)(2,1)} %constant_dynamic-update-slice_fusion, f32[512]{0:T(512)S(1)} %add_rsqrt_fusion), kind=kOutput, calls=%fused_computation.27 | convolution fusion | flops 2685665280 | bytes 8652800 | tf_op jit(solution)/shard_map/dot_general | solution.py:65
  42.1 21.9 %all_gather.22 = f32[4096,2]{0,1:T(2,128)S(1)} all-gather(f32[512,2]{0,1:T(2,128)S(1)} %copy-done.6), channel_id=1, replica_groups=mesh['sp'=8,'tp'=4] {'sp'}, dimensions={0}, use_global_device_ids=true | all-gather | bytes 36864 | tf_op jit(solution)/shard_map/all_gather | solution.py:111
  64.0 5.8 %collective-permute-start = (bf16[3,256]{1,0:T(4,128)(2,1)S(1)}, bf16[3,256]{1,0:T(4,128)(2,1)S(1)}, u32[]{:S(2)}, u32[]{:S(2)}) collective-permute-start(bf16[3,256]{1,0:T(4,128)(2,1)S(1)} %slice.405), channel_id=1, source_target_pairs={{0,4},{4,8},{8,12},{12,16},{16,20},{20,24},{24,28},{1,5},{5,9},{9,... | collective-permute-start | bytes 4616 | tf_op jit(solution)/shard_map/ppermute | solution.py:19
  79.4 13.5 %all-gather.1 = f32[8,1,256]{2,1,0:T(1,128)S(1)} all-gather(f32[1,1,256]{2,1,0:T(1,128)S(1)} %add_bitcast_fusion), channel_id=1, replica_groups=mesh['sp'=8,'tp'=4] {'sp'}, dimensions={0}, use_global_device_ids=true | all-gather | bytes 9216 | tf_op jit(solution)/shard_map/all_gather | solution.py:24
  93.1 14.2 %all-gather = f32[8,1,256]{2,1,0:T(1,128)S(1)} all-gather(f32[1,1,256]{2,1,0:T(1,128)S(1)} %add_bitcast_fusion.1), channel_id=1, replica_groups=mesh['sp'=8,'tp'=4] {'sp'}, dimensions={0}, use_global_device_ids=true | all-gather | bytes 9216 | tf_op jit(solution)/shard_map/all_gather | solution.py:24
  109.1 3.0 %copy.46 = bf16[4,1024,256]{1,2,0:T(8,128)(2,1)S(1)} copy(bf16[4,1024,256]{2,1,0:T(8,128)(2,1)} %bitcast.72) | data formatting | bytes 4194304
  112.1 27.0 %all-gather.10.cloned.1.call-done = bf16[4096,256]{1,0:T(8,128)(2,1)} async-done(((bf16[512,256]{1,0:T(8,128)(2,1)}), bf16[4096,256]{1,0:T(8,128)(2,1)}) %all-gather.10.cloned.1.call-update) | async-done | bytes 2097168 | tf_op jit(solution)/shard_map/all_gather | solution.py:178
  139.1 4.0 %copy.48 = bf16[4,1024,256]{1,2,0:T(8,128)(2,1)} copy(bf16[4,1024,256]{2,1,0:T(8,128)(2,1)} %bitcast.73) | data formatting | bytes 4194304
  143.1 33.0 %while.28 = (s32[]{:T(128)}, f32[2,512]{1,0:T(2,128)S(1)}, f32[2,512]{1,0:T(2,128)S(1)}, f32[2,512,128]{2,1,0:T(8,128)S(1)}, s32[4]{0:T(128)S(1)}, /*index=5*/s3...) while((s32[]{:T(128)}, f32[2,512]{1,0:T(2,128)S(1)}, ...), condition=%wide.region_8.9_spmd.clone, body=%wide.region_3.8_spmd.clone.sunk | while | flops 557583872 | bytes 19272052 | solution.py:189
  144.4 7.0 %conditional.3 = ((f32[2,512]{1,0:T(2,128)S(1)}, f32[2,512]{1,0:T(2,128)S(1)}, f32[2,512,128]{2,1,0:T(8,128)S(1)})) conditional(s32[]{:T(128)} %convert_element_type.128, (f32[2,512]{1,0:T(2,128)S(1)}, f32[2,512]{1,0:T(2,128)S(1)}, f32[2,512,128]{2,1,0:T(8,128)S(1)}) %tuple.91, (s32[]{:T(128)}, s32[]{:T(128)}, bf16[4,1024,256]{1,2,0:T(8,128)(2,1)S(1)}, ...), branch_computations={%region_4.4_spmd, %region_5.7_spmd} | conditional | flops 557583872 | bytes 19269714 | solution.py:157
  146.0 1.5 fusion.4
  147.5 1.5 fusion.3
  149.0 2.4 %fusion.8 = f32[2,512,128]{2,1,0:T(8,128)S(1)} fusion(bf16[1024,2,128]{0,2,1:T(8,128)(2,1)S(1)} %bitcast.70, f32[2,1024,512]{2,1,0:T(8,128)S(1)} %get-tuple-element.320, f32[2,512]{1,0:T(2,128)S(1)} %max.10, f32[2,1024]{1,0:T(2,128)S(1)} %dynamic-slice_bitcast_fusion, f32[2,512]{1,0:T(2,128)S(1)} %get-tuple-element.185, ...), kind=kOutput, calls=%fused_computation.11 | convolution fusion | flops 276037632 | bytes 6311936 | tf_op jit(solution)/shard_map/while/body/eval_jaxpr/cond/branch_1_fun/hqk,khd->hqd/dot_general | solution.py:146
  152.6 7.0 %conditional.3 = ((f32[2,512]{1,0:T(2,128)S(1)}, f32[2,512]{1,0:T(2,128)S(1)}, f32[2,512,128]{2,1,0:T(8,128)S(1)})) conditional(s32[]{:T(128)} %convert_element_type.128, (f32[2,512]{1,0:T(2,128)S(1)}, f32[2,512]{1,0:T(2,128)S(1)}, f32[2,512,128]{2,1,0:T(8,128)S(1)}) %tuple.91, (s32[]{:T(128)}, s32[]{:T(128)}, bf16[4,1024,256]{1,2,0:T(8,128)(2,1)S(1)}, ...), branch_computations={%region_4.4_spmd, %region_5.7_spmd} | conditional | flops 557583872 | bytes 19269714 | solution.py:157
  154.2 1.5 fusion.4
  155.7 1.5 fusion.3
  157.2 2.4 %fusion.8 = f32[2,512,128]{2,1,0:T(8,128)S(1)} fusion(bf16[1024,2,128]{0,2,1:T(8,128)(2,1)S(1)} %bitcast.70, f32[2,1024,512]{2,1,0:T(8,128)S(1)} %get-tuple-element.320, f32[2,512]{1,0:T(2,128)S(1)} %max.10, f32[2,1024]{1,0:T(2,128)S(1)} %dynamic-slice_bitcast_fusion, f32[2,512]{1,0:T(2,128)S(1)} %get-tuple-element.185, ...), kind=kOutput, calls=%fused_computation.11 | convolution fusion | flops 276037632 | bytes 6311936 | tf_op jit(solution)/shard_map/while/body/eval_jaxpr/cond/branch_1_fun/hqk,khd->hqd/dot_general | solution.py:146
  160.9 7.0 %conditional.3 = ((f32[2,512]{1,0:T(2,128)S(1)}, f32[2,512]{1,0:T(2,128)S(1)}, f32[2,512,128]{2,1,0:T(8,128)S(1)})) conditional(s32[]{:T(128)} %convert_element_type.128, (f32[2,512]{1,0:T(2,128)S(1)}, f32[2,512]{1,0:T(2,128)S(1)}, f32[2,512,128]{2,1,0:T(8,128)S(1)}) %tuple.91, (s32[]{:T(128)}, s32[]{:T(128)}, bf16[4,1024,256]{1,2,0:T(8,128)(2,1)S(1)}, ...), branch_computations={%region_4.4_spmd, %region_5.7_spmd} | conditional | flops 557583872 | bytes 19269714 | solution.py:157
  162.5 1.5 fusion.4
  164.0 1.5 fusion.3
  165.5 2.4 %fusion.8 = f32[2,512,128]{2,1,0:T(8,128)S(1)} fusion(bf16[1024,2,128]{0,2,1:T(8,128)(2,1)S(1)} %bitcast.70, f32[2,1024,512]{2,1,0:T(8,128)S(1)} %get-tuple-element.320, f32[2,512]{1,0:T(2,128)S(1)} %max.10, f32[2,1024]{1,0:T(2,128)S(1)} %dynamic-slice_bitcast_fusion, f32[2,512]{1,0:T(2,128)S(1)} %get-tuple-element.185, ...), kind=kOutput, calls=%fused_computation.11 | convolution fusion | flops 276037632 | bytes 6311936 | tf_op jit(solution)/shard_map/while/body/eval_jaxpr/cond/branch_1_fun/hqk,khd->hqd/dot_general | solution.py:146
  169.2 7.0 %conditional.3 = ((f32[2,512]{1,0:T(2,128)S(1)}, f32[2,512]{1,0:T(2,128)S(1)}, f32[2,512,128]{2,1,0:T(8,128)S(1)})) conditional(s32[]{:T(128)} %convert_element_type.128, (f32[2,512]{1,0:T(2,128)S(1)}, f32[2,512]{1,0:T(2,128)S(1)}, f32[2,512,128]{2,1,0:T(8,128)S(1)}) %tuple.91, (s32[]{:T(128)}, s32[]{:T(128)}, bf16[4,1024,256]{1,2,0:T(8,128)(2,1)S(1)}, ...), branch_computations={%region_4.4_spmd, %region_5.7_spmd} | conditional | flops 557583872 | bytes 19269714 | solution.py:157
  170.8 1.5 fusion.4
  172.2 1.5 fusion.3
  173.8 2.4 %fusion.8 = f32[2,512,128]{2,1,0:T(8,128)S(1)} fusion(bf16[1024,2,128]{0,2,1:T(8,128)(2,1)S(1)} %bitcast.70, f32[2,1024,512]{2,1,0:T(8,128)S(1)} %get-tuple-element.320, f32[2,512]{1,0:T(2,128)S(1)} %max.10, f32[2,1024]{1,0:T(2,128)S(1)} %dynamic-slice_bitcast_fusion, f32[2,512]{1,0:T(2,128)S(1)} %get-tuple-element.185, ...), kind=kOutput, calls=%fused_computation.11 | convolution fusion | flops 276037632 | bytes 6311936 | tf_op jit(solution)/shard_map/while/body/eval_jaxpr/cond/branch_1_fun/hqk,khd->hqd/dot_general | solution.py:146
  176.4 4.2 %convolution_convert_fusion = bf16[2048,512]{1,0:T(8,128)(2,1)} fusion(bf16[256,2048]{1,0:T(8,128)(2,1)} %param.33, bf16[256,2048]{1,0:T(8,128)(2,1)} %param.32, bf16[512,256]{1,0:T(8,128)(2,1)S(1)} %copy_bitcast_fusion, bf16[512,256]{1,0:T(8,128)(2,1)S(1)} %fusion.31), kind=kOutput, calls=%fused_computation.26 | convolution fusion | flops 1080033280 | bytes 4718592 | tf_op jit(solution)/shard_map/dot_general | solution.py:206
  180.6 31.7 %reduce-scatter.2.cloned.1.call-done = bf16[512,512]{1,0:T(8,128)(2,1)} async-done(((bf16[2048,512]{1,0:T(8,128)(2,1)}), bf16[512,512]{1,0:T(8,128)(2,1)}) %reduce-scatter.2.cloned.1.call-update) | async-done | bytes 524304 | tf_op jit(solution)/shard_map/reduce_scatter | solution.py:205
  212.3 2.0 copy.50
  (246 shorter events, 25.0 us)
Async XLA Ops:
  6.5 64.7 %copy-start = (bf16[16,64,64]{2,1,0:T(8,128)(2,1)S(1)}, bf16[16,64,64]{2,1,0:T(8,128)(2,1)}, u32[]{:S(2)}) copy-start(bf16[16,64,64]{2,1,0:T(8,128)(2,1)} %param.27) | copy-start | bytes 393220
  6.5 5.6 %copy-start.2 = (bf16[2048,256]{1,0:T(8,128)(2,1)S(1)}, bf16[2048,256]{1,0:T(8,128)(2,1)}, u32[]{:S(2)}) copy-start(bf16[2048,256]{1,0:T(8,128)(2,1)} %param.23) | copy-start | bytes 3145732
  6.5 6.8 %copy-start.3 = (bf16[2048,256]{1,0:T(8,128)(2,1)S(1)}, bf16[2048,256]{1,0:T(8,128)(2,1)}, u32[]{:S(2)}) copy-start(bf16[2048,256]{1,0:T(8,128)(2,1)} %param.24) | copy-start | bytes 3145732
  6.5 26.3 %all-gather.6.cloned.1.call-start = ((), (), s32[]{:S(2)}) async-start(), calls=%async_computation.1 | async-start | bytes 2621440 | tf_op jit(solution)/shard_map/all_gather | solution.py:62
  7.3 7.2 %copy-start.4 = (bf16[2048,256]{1,0:T(8,128)(2,1)S(1)}, bf16[2048,256]{1,0:T(8,128)(2,1)}, u32[]{:S(2)}) copy-start(bf16[2048,256]{1,0:T(8,128)(2,1)} %param.25) | copy-start | bytes 3145732
  7.3 101.8 %all-gather.8.cloned.1.call-start = ((), (), s32[]{:S(2)}) async-start(), calls=%async_computation.2 | async-start | bytes 2359296 | tf_op jit(solution)/shard_map/all_gather | solution.py:177
  35.0 7.1 %copy-start.6 = (f32[512,2]{0,1:T(2,128)S(1)}, f32[512,2]{0,1:T(2,128)}, u32[]{:S(2)}) copy-start(f32[512,2]{0,1:T(2,128)} %param.31) | copy-start | bytes 12292
  35.0 29.0 %copy-start.7 = (bf16[4,1024]{1,0:T(4,128)(2,1)S(1)}, bf16[4,1024]{1,0:T(4,128)(2,1)}, u32[]{:S(2)}) copy-start(bf16[4,1024]{1,0:T(4,128)(2,1)} %param.26) | copy-start | bytes 24580
  41.0 29.8 %copy-start.1 = (bf16[512,1280]{1,0:T(8,128)(2,1)}, bf16[512,1280]{1,0:T(8,128)(2,1)S(1)}, u32[]{:S(2)}) copy-start(bf16[512,1280]{1,0:T(8,128)(2,1)S(1)} %fusion.15) | copy-start | bytes 3932164
  42.0 97.0 %all-gather.10.cloned.1.call-start = ((), (), s32[]{:S(2)}) async-start(), calls=%async_computation.3 | async-start | bytes 2359296 | tf_op jit(solution)/shard_map/all_gather | solution.py:178
  42.1 31.1 %copy-start.5 = (f32[512,256]{1,0:T(8,128)S(1)}, f32[512,256]{1,0:T(8,128)}, u32[]{:S(2)}) copy-start(f32[512,256]{1,0:T(8,128)} %param.30) | copy-start | bytes 1572868
  64.0 6.7 %collective-permute-start = (bf16[3,256]{1,0:T(4,128)(2,1)S(1)}, bf16[3,256]{1,0:T(4,128)(2,1)S(1)}, u32[]{:S(2)}, u32[]{:S(2)}) collective-permute-start(bf16[3,256]{1,0:T(4,128)(2,1)S(1)} %slice.405), channel_id=1, source_target_pairs={{0,4},{4,8},{8,12},{12,16},{16,20},{20,24},{24,28},{1,5},{5,9},{9,... | collective-permute-start | bytes 4616 | tf_op jit(solution)/shard_map/ppermute | solution.py:19
  70.7 141.6 %reduce-scatter.2.cloned.1.call-start = ((), (), s32[]{:S(2)}) async-start(), calls=%async_computation.4 | async-start | bytes 2621440 | tf_op jit(solution)/shard_map/reduce_scatter | solution.py:205
Sparse Core Ops, SparseCore 0:
  8.9 23.9 all-gather.5
  42.1 46.7 all-gather.7
  91.1 47.9 all-gather.9
  180.7 31.5 reduce-scatter.1
where the time goes:
time: 224 us; the launch traced here: 221 us
  waiting for transfers between devices  76.8 us (34%)
  blocking collectives  49.5 us (22%)
  local copies, waits for them, and re-layouts  30.5 us (14%)
  matrix products  27.1 us (12%)
  between operations  14.1 us (6%)
  other arithmetic  13.4 us (6%)
  starting transfers between devices  5.97 us (3%)
  loops' own time  3.38 us (2%)
    reduce_scatter x1, waiting for transfers between devices, shards(): lax.psum_scatter(lax.dot_general(weight_part, branch, (((0,), (1,)), ((),...  31.7 us
    all_gather x2, blocking collectives, entering(): gathered = jax.tree.map(lambda a: lax.all_gather(a, axis), part)  27.7 us
    all_gather x1, waiting for transfers between devices, shards(): value_rows = lax.all_gather(values_dev, 'sp', axis=0, tiled=True)  27 us
    all_gather x1, blocking collectives, shards(): gates_all = lax.all_gather(forget_cum, 'sp', axis=0, tiled=True)  21.9 us
    all_gather x1, waiting for transfers between devices, shards(): portion = lax.all_gather(tokens, 'tp', axis=1, tiled=True)  17.3 us
    unnamed x24, local copies, waits for them, and re-layouts  14.2 us
    dot_general x4, matrix products, active(): jnp.einsum('hqk,khd->hqd', probs.astype(jnp.bfloat16), value_heads, prefe...  9.44 us
    dynamic_slice x8, local copies, waits for them, and re-layouts, shards(): lax.scan(visit_block, attn_start, (key_blocks, value_blocks, jnp.arange(b...  6.82 us
  transfers between devices with their start and end apart: 5, of which 3 were waited for; matrix products, arithmetic and copies ran while one was open for 10% of the time, Pallas kernels for 0%

commit v1 on v0

v1 whole, which is shorter than its diff:
```python
import functools

import jax
import jax.numpy as jnp
from jax import lax
from jax.experimental import pallas as pl
from jax.experimental.pallas import tpu as pltpu
from jax.sharding import PartitionSpec as P

HEAD_DIM = 128
decay_sharpness = 8.0
epsilon_norm = 1e-06
MESH = pl.DeviceIdType.MESH
F32 = jnp.float32
BF16 = jnp.bfloat16


def one_minus_exp(w):
    u = -w
    series = 1.0 - u / 9.0
    for n in range(8, 1, -1):
        series = 1.0 - u / n * series
    return jnp.where(u < 0.5, u * series, 1.0 - jnp.exp(w))


def remote(src, dst, send_sem, recv_sem, device):
    return pltpu.make_async_remote_copy(
        src_ref=src,
        dst_ref=dst,
        send_sem=send_sem,
        recv_sem=recv_sem,
        device_id=device,
        device_id_type=MESH,
    )


def kernel(
    SP,
    TP,
    X,
    tokens,
    lru_in,
    gate_in,
    query_w,
    key_w,
    value_w,
    conv_w,
    rg_w,
    ig_w,
    rate,
    decay_extra,
    forget,
    out_lru,
    out_fox,
    out,
    tok_buf,
    w_buf,
    acc,
    sq,
    lru_ref,
    halo,
    pad,
    bd_r,
    bd_i,
    gate_ref,
    q_ref,
    decay_buf,
    prefix_ref,
    local_ref,
    ends,
    incoming,
    kv_buf,
    cum_buf,
    cum_pad,
    m_ref,
    l_ref,
    o_ref,
    wl_buf,
    wf_buf,
    br_lru,
    br_fox,
    oacc,
    load_sem,
    tsend,
    tfwd,
    trecv,
    hsend,
    hrecv,
    esend,
    erecv,
    zsend,
    xsend,
    kvrecv,
    wsend,
    wrecv,
    lsend,
    lrecv,
    fsend,
    ffwd,
    frecv,
):
    rows, dcols = tokens.shape
    D, lw = lru_in.shape
    fw = query_w.shape[1]
    H = fw // HEAD_DIM
    oc = out.shape[1]
    Y = TP // 2
    Z = SP // X
    CH = tsend.shape[1]
    rc = rows // CH
    sp = lax.axis_index("sp")
    tp = lax.axis_index("tp")
    z = lax.div(sp, X)
    x = lax.rem(sp, X)
    partner = tp + 1 - 2 * lax.rem(tp, 2)
    far = [lax.rem(tp + 2 * k, TP) for k in range(Y)]
    pfar = [lax.rem(partner + 2 * k, TP) for k in range(Y)]
    offs = [0, lw, lw + fw, lw + 2 * fw, 2 * lw + 2 * fw, 2 * lw + 3 * fw]

    barrier = pltpu.get_barrier_semaphore()
    for k in range(1, SP):
        pl.semaphore_signal(
            barrier, inc=1, device_id={"sp": lax.rem(sp + k, SP)}, device_id_type=MESH
        )
    for k in range(1, TP):
        pl.semaphore_signal(
            barrier, inc=1, device_id={"tp": lax.rem(tp + k, TP)}, device_id_type=MESH
        )
    loads = []
    for i, w in enumerate((lru_in, key_w, value_w, gate_in, query_w)):
        c = pltpu.make_async_copy(w, w_buf.at[:, offs[i] : offs[i + 1]], load_sem.at[i])
        c.start()
        loads.append(c)
    mine = pl.ds(pl.multiple_of(tp * oc, 128), oc)
    own_loads = [
        pltpu.make_async_copy(decay_extra, decay_buf, load_sem.at[5]),
        pltpu.make_async_copy(out_lru.at[:, mine], wl_buf.at[tp], load_sem.at[6]),
        pltpu.make_async_copy(out_fox.at[:, mine], wf_buf.at[tp], load_sem.at[7]),
    ]
    for c in own_loads:
        c.start()
    pl.semaphore_wait(barrier, SP - 1 + TP - 1)

    pending = []

    def chunk(c):
        return pl.ds(c * rc, rc)

    for c in range(CH):
        for k in range(1, Y):
            s = remote(
                tokens.at[chunk(c)],
                tok_buf.at[tp, chunk(c)],
                tsend.at[k, c],
                trecv.at[tp, c],
                {"tp": far[k]},
            )
            s.start()
            pending.append(s)
    for c in range(CH):
        s = remote(
            tokens.at[chunk(c)],
            tok_buf.at[tp, chunk(c)],
            tsend.at[0, c],
            trecv.at[tp, c],
            {"tp": partner},
        )
        s.start()
        pending.append(s)

    bw = rg_w.shape[1]
    nb = lw // bw
    bd_r[...] = jnp.zeros_like(bd_r)
    bd_i[...] = jnp.zeros_like(bd_i)
    for n in range(nb):
        sl = pl.ds(n * bw, bw)
        bd_r[sl, sl] = rg_w[tp * nb + n]
        bd_i[sl, sl] = ig_w[tp * nb + n]
    cum_pad[...] = jnp.zeros_like(cum_pad)
    cum_pad[:, 0:H] = forget[...]
    cum_buf[sp] = cum_pad[...].T[0:8, :]

    for c in loads:
        c.wait()

    def project(val, src, r, first=False):
        w_rows = pl.ds(pl.multiple_of(src * dcols, dcols), dcols)
        v32 = val.astype(F32)
        part = jnp.sum(v32 * v32, axis=1, keepdims=True)
        dot = jnp.dot(val, w_buf[w_rows, :], preferred_element_type=F32)
        if first:
            sq[r, :] = part
            acc[r, :] = dot
        else:
            sq[r, :] += part
            acc[r, :] += dot

    def tok_wait(src, c):
        ref = tok_buf.at[src, chunk(c)]
        remote(ref, ref, tsend.at[0, c], trecv.at[src, c], {"tp": partner}).wait_recv()

    for c in range(CH):
        project(tokens[chunk(c), :], tp, chunk(c), True)
    for c in range(CH):
        tok_wait(partner, c)
        project(tok_buf[partner, chunk(c), :], partner, chunk(c))
    for c in range(CH):
        for k in range(1, Y):
            tok_wait(far[k], c)
            ref = tok_buf.at[far[k], chunk(c)]
            s = remote(ref, ref, tfwd.at[k, c], trecv.at[far[k], c], {"tp": partner})
            s.start()
            pending.append(s)
            project(tok_buf[far[k], chunk(c), :], far[k], chunk(c))
        for k in range(1, Y):
            tok_wait(pfar[k], c)
            project(tok_buf[pfar[k], chunk(c), :], pfar[k], chunk(c))

    row_scale = lax.rsqrt(sq[...] / D + epsilon_norm)

    def scaled(i, n=1):
        return (acc[:, offs[i] : offs[i + n]] * row_scale).astype(BF16)

    lru_ref[...] = scaled(0)
    hb = halo.shape[0]
    halo_copy = remote(
        lru_ref.at[pl.ds(rows - hb, hb)],
        halo,
        hsend.at[0],
        hrecv.at[0],
        {"sp": lax.rem(sp + 1, SP)},
    )

    @pl.when(sp < SP - 1)
    def _():
        halo_copy.start()

    kv_buf[sp] = scaled(1, 2)

    def block_copies(j, a, send_sem, device):
        return (
            remote(kv_buf.at[j], kv_buf.at[j], send_sem.at[a, 0], kvrecv.at[j, 0], device),
            remote(cum_buf.at[j], cum_buf.at[j], send_sem.at[a, 1], kvrecv.at[j, 1], device),
        )

    def z_copies(dz):
        j = (z - dz) * X + x
        return block_copies(j, dz, zsend, {"sp": lax.rem(sp + X, SP)})

    def x_copies(dz, dx):
        j = (z - dz) * X + x
        xo = lax.rem(x + dx, X)
        return block_copies(j, dz, xsend.at[dx - 1], {"sp": z * X + xo})

    def for_sends(dz, own, act):
        @pl.when(z < Z - 1)
        def _():
            for c in z_copies(dz):
                act(c)

        for dx in range(1, X):
            if own:

                @pl.when(lax.rem(x + dx, X) > x)
                def _():
                    for c in x_copies(dz, dx):
                        act(c)
            else:
                for c in x_copies(dz, dx):
                    act(c)

    def kv_wait(j):
        for c in block_copies(j, 0, zsend, {"sp": lax.rem(sp + X, SP)}):
            c.wait_recv()

    for_sends(0, True, lambda c: c.start())

    for k in range(1, TP):
        t = lax.rem(tp + k, TP)
        cols = pl.ds(pl.multiple_of(t * oc, 128), oc)
        for i, (w, buf) in enumerate(((out_lru, wl_buf), (out_fox, wf_buf))):
            s = remote(w.at[:, cols], buf.at[tp], wsend.at[i, k], wrecv.at[i, tp], {"tp": t})
            s.start()
            pending.append(s)

    gate_ref[...] = scaled(3)
    q_ref[...] = scaled(4)

    @pl.when(sp == 0)
    def _():
        pad[0:8, :] = jnp.zeros((8, lw), F32)

    @pl.when(sp > 0)
    def _():
        halo_copy.wait_recv()
        pad[0:8, :] = halo[...].astype(F32)[hb - 8 : hb, :]

    pad[8 : 8 + rows, :] = lru_ref[...].astype(F32)
    chans = pl.ds(pl.multiple_of(tp * lw, 128), lw)
    taps = conv_w.shape[0]
    taps_f32 = conv_w[:, chans].astype(F32)
    conv = jnp.zeros((rows, lw), F32)
    for j in range(taps):
        conv = conv + taps_f32[j : j + 1, :] * pad[8 - (taps - 1) + j : 8 - (taps - 1) + j + rows, :]
    conv_b = conv.astype(BF16)

    def sigmoid(v):
        return 1.0 / (1.0 + jnp.exp(-v))

    recur_gate = sigmoid(jnp.dot(conv_b, bd_r[...], preferred_element_type=F32))
    input_gate = sigmoid(jnp.dot(conv_b, bd_i[...], preferred_element_type=F32))
    own_rate = rate[:, chans]
    softplus = jnp.maximum(-own_rate, 0.0) + jnp.log1p(jnp.exp(-jnp.abs(own_rate)))
    for c in own_loads:
        c.wait()
    log_decay = -decay_sharpness * softplus * recur_gate + decay_buf[...]
    prefix_ref[...] = jnp.exp(log_decay)
    local_ref[...] = jnp.sqrt(one_minus_exp(2.0 * log_decay)) * input_gate * conv_b.astype(F32)
    row_id = lax.broadcasted_iota(jnp.int32, (rows, lw), 0)
    step = 1
    while step < rows:
        a = prefix_ref[...]
        b = local_ref[...]
        keep = row_id >= step
        a_prev = jnp.where(keep, pltpu.roll(a, step, 0), 1.0)
        b_prev = jnp.where(keep, pltpu.roll(b, step, 0), 0.0)
        local_ref[...] = b + a * b_prev
        prefix_ref[...] = a * a_prev
        step *= 2
    ends[sp, 0:1, :] = prefix_ref[rows - 1 : rows, :]
    ends[sp, 1:2, :] = local_ref[rows - 1 : rows, :]

    def end_copy(k):
        return remote(
            ends.at[sp], ends.at[sp], esend.at[k], erecv.at[sp], {"sp": lax.rem(sp + k, SP)}
        )

    for k in range(1, SP):

        @pl.when(sp + k < SP)
        def _():
            end_copy(k).start()

    score_scale = HEAD_DIM ** (-0.5)
    qc = rc

    def attend(j, diagonal):
        def some(i, carry):
            r = pl.ds(pl.multiple_of(i * qc, qc), qc)
            for h in range(H):
                hs = slice(h * HEAD_DIM, (h + 1) * HEAD_DIM)
                vs = slice(fw + h * HEAD_DIM, fw + (h + 1) * HEAD_DIM)
                s = lax.dot_general(
                    q_ref[r, hs],
                    kv_buf[j, :, hs],
                    (((1,), (1,)), ((), ())),
                    preferred_element_type=F32,
                )
                s = s * score_scale + forget[r, h : h + 1] - cum_buf[j, h : h + 1, :]
                if diagonal:
                    causal = (
                        lax.broadcasted_iota(jnp.int32, (qc, rows), 0) + i * qc
                        >= lax.broadcasted_iota(jnp.int32, (qc, rows), 1)
                    )
                    s = jnp.where(causal, s, -1e30)
                top = jnp.max(s, axis=1, keepdims=True)
                if diagonal:
                    p = jnp.exp(s - top)
                    m_ref[h, r, :] = top
                    l_ref[h, r, :] = jnp.sum(p, axis=1, keepdims=True)
                    o_ref[h, r, :] = jnp.dot(
                        p.astype(BF16), kv_buf[j, :, vs], preferred_element_type=F32
                    )
                else:
                    old = m_ref[h, r, :]
                    new = jnp.maximum(old, top)
                    p = jnp.exp(s - new)
                    fade = jnp.exp(old - new)
                    m_ref[h, r, :] = new
                    l_ref[h, r, :] = l_ref[h, r, :] * fade + jnp.sum(p, axis=1, keepdims=True)
                    o_ref[h, r, :] = o_ref[h, r, :] * fade + jnp.dot(
                        p.astype(BF16), kv_buf[j, :, vs], preferred_element_type=F32
                    )
            return carry

        lax.fori_loop(0, rows // qc, some, 0)

    attend(sp, True)

    def row_blocks(dz):
        for dx in range(1, X):
            xo = lax.rem(x + dx, X)

            @pl.when(jnp.logical_or(dz > 0, xo < x))
            def _():
                j = (z - dz) * X + xo
                kv_wait(j)
                attend(j, False)

    def finish_lru():
        incoming[...] = jnp.zeros_like(incoming)
        for j in range(SP - 1):

            @pl.when(j < sp)
            def _():
                remote(
                    ends.at[j], ends.at[j], esend.at[0], erecv.at[j], {"sp": lax.rem(sp + 1, SP)}
                ).wait_recv()
                incoming[...] = ends[j, 0:1, :] * incoming[...] + ends[j, 1:2, :]

        states = local_ref[...] + prefix_ref[...] * incoming[...]
        g = gate_ref[...].astype(F32)
        gelu = 0.5 * g * (1.0 + jnp.tanh(0.7978845608028654 * (g + 0.044715 * (g * g * g))))
        br_lru[tp] = (states * gelu).astype(BF16)
        for k in range(1, TP):
            lru_copy(k).start()

    def lru_copy(k):
        t = lax.rem(tp + k, TP)
        return remote(br_lru.at[tp], br_lru.at[tp], lsend.at[k], lrecv.at[tp], {"tp": t})

    lru_step = min(2, Z - 1)
    if Z == 1:
        finish_lru()

    def hop(dz, carry):
        @pl.when(dz <= z)
        def _():
            j = (z - dz) * X + x
            kv_wait(j)
            for_sends(dz, False, lambda c: c.start())
            row_blocks(dz - 1)
            attend(j, False)

        @pl.when(dz == lru_step)
        def _():
            finish_lru()

        return carry

    lax.fori_loop(1, Z, hop, 0)

    for k in range(TP):
        t = lax.rem(tp + k, TP)
        if k > 0:
            for i, buf in enumerate((wl_buf, wf_buf)):
                remote(buf.at[t], buf.at[t], wsend.at[i, k], wrecv.at[i, t], {"tp": t}).wait_recv()
            remote(br_lru.at[t], br_lru.at[t], lsend.at[k], lrecv.at[t], {"tp": t}).wait_recv()
        dot = jnp.dot(br_lru[t], wl_buf[t], preferred_element_type=F32)
        if k == 0:
            oacc[...] = dot
        else:
            oacc[...] += dot

    row_blocks(z)

    for c in range(CH):
        r = chunk(c)
        for h in range(H):
            br_fox[tp, r, h * HEAD_DIM : (h + 1) * HEAD_DIM] = (
                o_ref[h, r, :] / l_ref[h, r, :]
            ).astype(BF16)
        ref = br_fox.at[tp, r]
        for k in list(range(1, Y)) + [0]:
            to = far[k] if k else partner
            s = remote(ref, ref, fsend.at[k, c], frecv.at[tp, c], {"tp": to})
            s.start()
            pending.append(s)

    def fox_wait(src, c):
        ref = br_fox.at[src, chunk(c)]
        remote(ref, ref, fsend.at[0, c], frecv.at[src, c], {"tp": partner}).wait_recv()

    def fox_dot(src, r):
        return jnp.dot(br_fox[src, r, :], wf_buf[src], preferred_element_type=F32)

    for c in range(CH):
        fox_wait(partner, c)
        oacc[chunk(c), :] += fox_dot(tp, chunk(c)) + fox_dot(partner, chunk(c))
    for c in range(CH):
        r = chunk(c)
        for k in range(1, Y):
            fox_wait(far[k], c)
            ref = br_fox.at[far[k], r]
            s = remote(ref, ref, ffwd.at[k, c], frecv.at[far[k], c], {"tp": partner})
            s.start()
            pending.append(s)
            oacc[r, :] += fox_dot(far[k], r)
        for k in range(1, Y):
            fox_wait(pfar[k], c)
            oacc[r, :] += fox_dot(pfar[k], r)
        out[r, :] = oacc[r, :].astype(out.dtype)

    for s in pending:
        s.wait_send()
    for k in range(1, TP):
        lru_copy(k).wait_send()

    @pl.when(sp < SP - 1)
    def _():
        halo_copy.wait_send()

    for k in range(1, SP):

        @pl.when(sp + k < SP)
        def _():
            end_copy(k).wait_send()

    for_sends(0, True, lambda c: c.wait_send())

    def drain(dz, carry):
        @pl.when(dz <= z)
        def _():
            for_sends(dz, False, lambda c: c.wait_send())

        return carry

    lax.fori_loop(1, Z, drain, 0)


def shards(SP, TP, X, *args):
    tokens, lru_in, gate_in, query_w = args[:4]
    (conv_weight, rg_w, ig_w, rate, decay_extra, forget, out_lru, out_fox) = args[6:]
    rows, dcols = tokens.shape
    D, lw = lru_in.shape
    fw = query_w.shape[1]
    oc = out_lru.shape[1] // TP
    tot = 2 * lw + 3 * fw
    H = fw // HEAD_DIM
    Y = TP // 2
    Z = SP // X
    CH = 2
    vm = pl.BlockSpec(memory_space=pltpu.VMEM)
    hbm = pl.BlockSpec(memory_space=pl.ANY)
    dma = pltpu.SemaphoreType.DMA
    V = pltpu.VMEM
    scratch = [
        V((TP, rows, dcols), BF16),
        V((D, tot), BF16),
        V((rows, tot), F32),
        V((rows, 1), F32),
        V((rows, lw), BF16),
        V((16, lw), BF16),
        V((rows + 8, lw), F32),
        V((lw, lw), BF16),
        V((lw, lw), BF16),
        V((rows, lw), BF16),
        V((rows, fw), BF16),
        V((rows, lw), F32),
        V((rows, lw), F32),
        V((rows, lw), F32),
        V((SP, 8, lw), F32),
        V((1, lw), F32),
        V((SP, rows, 2 * fw), BF16),
        V((SP, 8, rows), F32),
        V((rows, 128), F32),
        V((H, rows, 1), F32),
        V((H, rows, 1), F32),
        V((H, rows, HEAD_DIM), F32),
        V((TP, lw, oc), BF16),
        V((TP, fw, oc), BF16),
        V((TP, rows, lw), BF16),
        V((TP, rows, fw), BF16),
        V((rows, oc), F32),
        dma((8,)),
        dma((Y, CH)),
        dma((Y, CH)),
        dma((TP, CH)),
        dma((1,)),
        dma((1,)),
        dma((SP,)),
        dma((SP,)),
        dma((Z, 2)),
        dma((max(X - 1, 1), Z, 2)),
        dma((SP, 2)),
        dma((2, TP)),
        dma((2, TP)),
        dma((TP,)),
        dma((TP,)),
        dma((Y, CH)),
        dma((Y, CH)),
        dma((TP, CH)),
    ]
    return pl.pallas_call(
        functools.partial(kernel, SP, TP, X),
        out_shape=jax.ShapeDtypeStruct((rows, oc), BF16),
        in_specs=[vm] + [hbm] * 5 + [vm] * 4 + [hbm, vm, hbm, hbm],
        out_specs=vm,
        scratch_shapes=scratch,
        compiler_params=pltpu.CompilerParams(
            collective_id=0, has_side_effects=True, vmem_limit_bytes=60 * 1024 * 1024
        ),
    )(*args[:9], rate.reshape(1, -1), decay_extra, forget, out_lru, out_fox)


def columns_of(mesh):
    SP = mesh.shape["sp"]
    try:
        X = len({d.coords[0] for d in mesh.devices.flat})
    except AttributeError:
        X = 2
    return X if SP % X == 0 else 1


def solution(mesh):
    placed = (
        P("sp", "tp"),
        P(None, "tp"),
        P(None, "tp"),
        P(None, "tp"),
        P(None, "tp"),
        P(None, "tp"),
        P(),
        P(),
        P(),
        P(),
        P("sp", "tp"),
        P("sp", "tp"),
        P("tp", None),
        P("tp", None),
    )
    body = functools.partial(shards, mesh.shape["sp"], mesh.shape["tp"], columns_of(mesh))
    return jax.shard_map(
        body, mesh=mesh, in_specs=placed, out_specs=P("sp", "tp"), check_vma=False
    )
```

time: 224 us -> 87.9 us (0.39); the launches traced: 221 us -> 87.7 us
  Pallas kernels: 0 us -> 84.2 us
  waiting for transfers between devices: 76.8 us -> 0 us
  blocking collectives: 49.5 us -> 0 us
  matrix products: 27.1 us -> 0 us
  local copies, waits for them, and re-layouts: 30.5 us -> 3.41 us
  between operations: 14.1 us -> 0.01 us
  other arithmetic: 13.4 us -> 0 us
  starting transfers between devices: 5.97 us -> 0 us
  loops' own time: 3.38 us -> 0 us
    pallas_call x0 -> x1, Pallas kernels: none -> 84.2 us  [shards(): pl.pallas_call(functools.partial(kernel, SP, TP, X), out_shape=jax.ShapeD...]
    all_gather x3 -> x0, blocking collectives: 49.5 us -> none  [the longest x2 27.7 us: entering(): gathered = jax.tree.map(lambda a: lax.all_gather(a, axis), part)]
    all_gather x3 -> x0, waiting for transfers between devices: 44.3 us -> none  [the longest x1 27 us: shards(): value_rows = lax.all_gather(values_dev, 'sp', axis=0, tiled=True)]
    reduce_scatter x1 -> x0, waiting for transfers between devices: 31.7 us -> none  [shards(): lax.psum_scatter(lax.dot_general(weight_part, branch, (((0,), (1,)), ((),...]
    dot_general x12 -> x0, matrix products: 27.1 us -> none  [the longest x4 9.44 us: active(): jnp.einsum('hqk,khd->hqd', probs.astype(jnp.bfloat16), value_heads, prefe...]
    unnamed x24 -> x2, local copies, waits for them, and re-layouts: 14.2 us -> 3.41 us
    reduce_sum x5 -> x0, other arithmetic: 8.05 us -> none  [the longest x4 5.98 us: active(): new_totals = totals * rescale + jnp.sum(probs, axis=2)]
    dynamic_slice x14 -> x0, local copies, waits for them, and re-layouts: 6.87 us -> none  [the longest x8 6.82 us: shards(): lax.scan(visit_block, attn_start, (key_blocks, value_blocks, jnp.arange(b...]
  transfers between devices with their start and end apart: 5 -> 0, of which waited for: 3 -> 0; matrix products, arithmetic and copies ran while one was open for 10% -> 0% of each run, Pallas kernels for 0% -> 0%
where the time goes in v1:
time: 87.9 us; the launch traced here: 87.7 us
  Pallas kernels  84.2 us (96%)
  local copies, waits for them, and re-layouts  3.41 us (4%)
    pallas_call x1, Pallas kernels, shards(): pl.pallas_call(functools.partial(kernel, SP, TP, X), out_shape=jax.ShapeD...  84.2 us
    unnamed x2, local copies, waits for them, and re-layouts  3.41 us

profile of v1, /device:TPU:25, one launch (start us, length us, event | category | flops | bytes accessed | tf_op | source)
XLA Modules:
  0.0 87.7 jit_solution(8025608277402348177)
XLA Ops:
  0.0 1.5 %copy.15.forget = f32[512,2]{1,0:T(8,128)} copy(f32[512,2]{0,1:T(2,128)} %param.25) | data formatting | bytes 8192 | tf_op args[11]
  1.5 84.2 %shard_map.136 = bf16[512,512]{1,0:T(8,128)(2,1)} custom-call(bf16[512,512]{1,0:T(8,128)(2,1)} %tokens.1, bf16[2048,256]{1,0:T(8,128)(2,1)} %lru_in.1, bf16[2048,256]{1,0:T(8,128)(2,1)} %gate_in.1, bf16[2048,256]{1,0:T(8,128)(2,1)} %query_w.1, bf16[2048,256]{1,0:T(8,128)(2,1)} %key_w.1, bf16[2048,256]{1,0:T(8,128)(2,1)} %value_w.1, bf16[4,1024]{1,0:T(4,128)(2,1)} %conv_w.1, ...), custom_call_target="tpu_custom_call" | custom-call | tf_op jit(solution)/shard_map/pallas_call | solution.py:584
  85.8 1.9 %copy.17 = bf16[512,512]{1,0:T(8,128)(2,1)} copy(bf16[512,512]{1,0:T(8,128)(2,1)} %shard_map.136) | data formatting | bytes 1048576

commit v2 on v1

--- a/solution.py
+++ b/solution.py
@@ -72,9 +72,19 @@
     kv_buf,
     cum_buf,
     cum_pad,
+    wide,
+    fcol,
     m_ref,
     l_ref,
     o_ref,
+    q_far,
+    m_far,
+    l_far,
+    o_far,
+    part_out,
+    stat_out,
+    part_in,
+    stat_in,
     wl_buf,
     wf_buf,
     br_lru,
@@ -98,6 +108,11 @@
     fsend,
     ffwd,
     frecv,
+    lfwd,
+    qsend,
+    qrecv,
+    osend,
+    orecv,
 ):
     rows, dcols = tokens.shape
     D, lw = lru_in.shape
@@ -177,8 +192,10 @@
         bd_r[sl, sl] = rg_w[tp * nb + n]
         bd_i[sl, sl] = ig_w[tp * nb + n]
     cum_pad[...] = jnp.zeros_like(cum_pad)
-    cum_pad[:, 0:H] = forget[...]
-    cum_buf[sp] = cum_pad[...].T[0:8, :]
+    wide[...] = jnp.zeros_like(wide)
+    wide[0:H, :] = forget[...]
+    fcol[...] = wide[...].T
+    cum_buf[sp] = wide[0:8, :]
 
     for c in loads:
         c.wait()
@@ -237,6 +254,10 @@
 
     kv_buf[sp] = scaled(1, 2)
 
+    paired = Z in (3, 4)
+    helper = jnp.logical_and(z <= Z - 3, paired)
+    helped = jnp.logical_and(z >= 2, paired)
+
     def block_copies(j, a, send_sem, device):
         return (
             remote(kv_buf.at[j], kv_buf.at[j], send_sem.at[a, 0], kvrecv.at[j, 0], device),
@@ -253,15 +274,17 @@
         return block_copies(j, dz, xsend.at[dx - 1], {"sp": z * X + xo})
 
     def for_sends(dz, own, act):
-        @pl.when(z < Z - 1)
-        def _():
-            for c in z_copies(dz):
-                act(c)
+        if own or not paired:
+
+            @pl.when(z < Z - 1)
+            def _():
+                for c in z_copies(dz):
+                    act(c)
 
         for dx in range(1, X):
             if own:
 
-                @pl.when(lax.rem(x + dx, X) > x)
+                @pl.when(jnp.logical_or(lax.rem(x + dx, X) > x, helper))
                 def _():
                     for c in x_copies(dz, dx):
                         act(c)
@@ -275,16 +298,24 @@
 
     for_sends(0, True, lambda c: c.start())
 
-    for k in range(1, TP):
-        t = lax.rem(tp + k, TP)
-        cols = pl.ds(pl.multiple_of(t * oc, 128), oc)
-        for i, (w, buf) in enumerate(((out_lru, wl_buf), (out_fox, wf_buf))):
+    q_ref[...] = scaled(4)
+    q_copy = remote(
+        q_ref, q_far, qsend.at[0], qrecv.at[0], {"sp": lax.rem(sp + SP - 2 * X, SP)}
+    )
+
+    @pl.when(helped)
+    def _():
+        q_copy.start()
+
+    for i, (w, buf) in enumerate(((out_lru, wl_buf), (out_fox, wf_buf))):
+        for k in range(1, TP):
+            t = lax.rem(tp + k, TP)
+            cols = pl.ds(pl.multiple_of(t * oc, 128), oc)
             s = remote(w.at[:, cols], buf.at[tp], wsend.at[i, k], wrecv.at[i, tp], {"tp": t})
             s.start()
             pending.append(s)
 
     gate_ref[...] = scaled(3)
-    q_ref[...] = scaled(4)
 
     @pl.when(sp == 0)
     def _():
@@ -344,19 +375,26 @@
     score_scale = HEAD_DIM ** (-0.5)
     qc = rc
 
-    def attend(j, diagonal):
+    def attend(j, diagonal, far_first=None):
+        other = far_first is not None
+        first = diagonal or far_first
+        qs, ms, ls, os = (q_far, m_far, l_far, o_far) if other else (q_ref, m_ref, l_ref, o_ref)
+
         def some(i, carry):
             r = pl.ds(pl.multiple_of(i * qc, qc), qc)
             for h in range(H):
                 hs = slice(h * HEAD_DIM, (h + 1) * HEAD_DIM)
                 vs = slice(fw + h * HEAD_DIM, fw + (h + 1) * HEAD_DIM)
                 s = lax.dot_general(
-                    q_ref[r, hs],
+                    qs[r, hs],
                     kv_buf[j, :, hs],
                     (((1,), (1,)), ((), ())),
                     preferred_element_type=F32,
                 )
-                s = s * score_scale + forget[r, h : h + 1] - cum_buf[j, h : h + 1, :]
+                s = s * score_scale
+                if not other:
+                    s = s + fcol[r, h : h + 1]
+                s = s - cum_buf[j, h : h + 1, :]
                 if diagonal:
                     causal = (
                         lax.broadcasted_iota(jnp.int32, (qc, rows), 0) + i * qc
@@ -364,21 +402,21 @@
                     )
                     s = jnp.where(causal, s, -1e30)
                 top = jnp.max(s, axis=1, keepdims=True)
-                if diagonal:
+                if first:
                     p = jnp.exp(s - top)
-                    m_ref[h, r, :] = top
-                    l_ref[h, r, :] = jnp.sum(p, axis=1, keepdims=True)
-                    o_ref[h, r, :] = jnp.dot(
+                    ms[h, r, :] = top
+                    ls[h, r, :] = jnp.sum(p, axis=1, keepdims=True)
+                    os[h, r, :] = jnp.dot(
                         p.astype(BF16), kv_buf[j, :, vs], preferred_element_type=F32
                     )
                 else:
-                    old = m_ref[h, r, :]
+                    old = ms[h, r, :]
                     new = jnp.maximum(old, top)
                     p = jnp.exp(s - new)
                     fade = jnp.exp(old - new)
-                    m_ref[h, r, :] = new
-                    l_ref[h, r, :] = l_ref[h, r, :] * fade + jnp.sum(p, axis=1, keepdims=True)
-                    o_ref[h, r, :] = o_ref[h, r, :] * fade + jnp.dot(
+                    ms[h, r, :] = new
+                    ls[h, r, :] = ls[h, r, :] * fade + jnp.sum(p, axis=1, keepdims=True)
+                    os[h, r, :] = os[h, r, :] * fade + jnp.dot(
                         p.astype(BF16), kv_buf[j, :, vs], preferred_element_type=F32
                     )
             return carry
@@ -412,12 +450,12 @@
         g = gate_ref[...].astype(F32)
         gelu = 0.5 * g * (1.0 + jnp.tanh(0.7978845608028654 * (g + 0.044715 * (g * g * g))))
         br_lru[tp] = (states * gelu).astype(BF16)
-        for k in range(1, TP):
+        for k in range(Y - 1, -1, -1):
             lru_copy(k).start()
 
     def lru_copy(k):
-        t = lax.rem(tp + k, TP)
-        return remote(br_lru.at[tp], br_lru.at[tp], lsend.at[k], lrecv.at[tp], {"tp": t})
+        to = far[k] if k else partner
+        return remote(br_lru.at[tp], br_lru.at[tp], lsend.at[k], lrecv.at[tp], {"tp": to})
 
     lru_step = min(2, Z - 1)
     if Z == 1:
@@ -438,21 +476,127 @@
 
         return carry
 
-    lax.fori_loop(1, Z, hop, 0)
-
-    for k in range(TP):
+    up = {"sp": lax.rem(sp + 2 * X, SP)}
+    part_copies = (
+        remote(part_out, part_in, osend.at[0], orecv.at[0], up),
+        remote(stat_out, stat_in, osend.at[1], orecv.at[1], up),
+    )
+
+    def send_partial():
+        for h in range(H):
+            part_out[:, h * HEAD_DIM : (h + 1) * HEAD_DIM] = o_far[h].astype(BF16)
+            cum_pad[:, h : h + 1] = m_far[h]
+            cum_pad[:, H + h : H + h + 1] = l_far[h]
+        stat_out[...] = cum_pad[...].T[0:8, :]
+        for c in part_copies:
+            c.start()
+
+    if paired:
+        below = (z - 1) * X
+
+        @pl.when(helper)
+        def _():
+            q_copy.wait_recv()
+            attend(sp, False, True)
+
+        @pl.when(z >= 1)
+        def _():
+            kv_wait(below + x)
+            for_sends(1, False, lambda c: c.start())
+
+        for dx in range(1, X):
+            xo = lax.rem(x + dx, X)
+
+            @pl.when(jnp.logical_or(xo < x, helper))
+            def _():
+                kv_wait(z * X + xo)
+
+            @pl.when(helper)
+            def _():
+                attend(z * X + xo, False, False)
+
+        @pl.when(jnp.logical_and(helper, z == 0))
+        def _():
+            send_partial()
+
+        for dx in range(1, X):
+            xo = lax.rem(x + dx, X)
+
+            @pl.when(xo < x)
+            def _():
+                attend(z * X + xo, False)
+
+        finish_lru()
+
+        @pl.when(jnp.logical_and(helper, z >= 1))
+        def _():
+            attend(below + x, False, False)
+
+        @pl.when(z >= 1)
+        def _():
+            attend(below + x, False)
+            for dx in range(1, X):
+                j = below + lax.rem(x + dx, X)
+                kv_wait(j)
+
+                @pl.when(helper)
+                def _():
+                    attend(j, False, False)
+
+            @pl.when(helper)
+            def _():
+                send_partial()
+
+            for dx in range(1, X):
+                attend(below + lax.rem(x + dx, X), False)
+
+    else:
+        lax.fori_loop(1, Z, hop, 0)
+
+    def lru_wait(t):
+        remote(br_lru.at[t], br_lru.at[t], lsend.at[0], lrecv.at[t], {"tp": partner}).wait_recv()
+
+    def lru_dot(t):
+        return jnp.dot(br_lru[t], wl_buf[t], preferred_element_type=F32)
+
+    oacc[...] = lru_dot(tp)
+    for k in range(1, TP):
         t = lax.rem(tp + k, TP)
-        if k > 0:
-            for i, buf in enumerate((wl_buf, wf_buf)):
-                remote(buf.at[t], buf.at[t], wsend.at[i, k], wrecv.at[i, t], {"tp": t}).wait_recv()
-            remote(br_lru.at[t], br_lru.at[t], lsend.at[k], lrecv.at[t], {"tp": t}).wait_recv()
-        dot = jnp.dot(br_lru[t], wl_buf[t], preferred_element_type=F32)
-        if k == 0:
-            oacc[...] = dot
-        else:
-            oacc[...] += dot
-
-    row_blocks(z)
+        for i, buf in enumerate((wl_buf, wf_buf)):
+            remote(buf.at[t], buf.at[t], wsend.at[i, k], wrecv.at[i, t], {"tp": t}).wait_recv()
+    for k in range(1, Y):
+        lru_wait(far[k])
+        ref = br_lru.at[far[k]]
+        s = remote(ref, ref, lfwd.at[k], lrecv.at[far[k]], {"tp": partner})
+        s.start()
+        pending.append(s)
+    lru_wait(partner)
+    oacc[...] += lru_dot(partner)
+    for k in range(1, Y):
+        oacc[...] += lru_dot(far[k])
+        lru_wait(pfar[k])
+        oacc[...] += lru_dot(pfar[k])
+
+    if paired:
+
+        @pl.when(helped)
+        def _():
+            for c in part_copies:
+                c.wait_recv()
+            wide[0:8, :] = stat_in[...]
+            stats = wide[...].T
+            for h in range(H):
+                m_in = stats[:, h : h + 1] + fcol[:, h : h + 1]
+                l_in = stats[:, H + h : H + h + 1]
+                part = part_in[:, h * HEAD_DIM : (h + 1) * HEAD_DIM].astype(F32)
+                new = jnp.maximum(m_ref[h], m_in)
+                fade = jnp.exp(m_ref[h] - new)
+                grow = jnp.exp(m_in - new)
+                l_ref[h] = l_ref[h] * fade + l_in * grow
+                o_ref[h] = o_ref[h] * fade + part * grow
+
+    else:
+        row_blocks(z)
 
     for c in range(CH):
         r = chunk(c)
@@ -493,8 +637,17 @@
 
     for s in pending:
         s.wait_send()
-    for k in range(1, TP):
+    for k in range(Y):
         lru_copy(k).wait_send()
+
+    @pl.when(helped)
+    def _():
+        q_copy.wait_send()
+
+    @pl.when(helper)
+    def _():
+        for c in part_copies:
+            c.wait_send()
 
     @pl.when(sp < SP - 1)
     def _():
@@ -515,7 +668,14 @@
 
         return carry
 
-    lax.fori_loop(1, Z, drain, 0)
+    if paired:
+
+        @pl.when(z >= 1)
+        def _():
+            for_sends(1, False, lambda c: c.wait_send())
+
+    else:
+        lax.fori_loop(1, Z, drain, 0)
 
 
 def shards(SP, TP, X, *args):
@@ -554,9 +714,19 @@
         V((SP, rows, 2 * fw), BF16),
         V((SP, 8, rows), F32),
         V((rows, 128), F32),
+        V((128, rows), F32),
+        V((rows, 128), F32),
         V((H, rows, 1), F32),
         V((H, rows, 1), F32),
         V((H, rows, HEAD_DIM), F32),
+        V((rows, fw), BF16),
+        V((H, rows, 1), F32),
+        V((H, rows, 1), F32),
+        V((H, rows, HEAD_DIM), F32),
+        V((rows, fw), BF16),
+        V((8, rows), F32),
+        V((rows, fw), BF16),
+        V((8, rows), F32),
         V((TP, lw, oc), BF16),
         V((TP, fw, oc), BF16),
         V((TP, rows, lw), BF16),
@@ -580,6 +750,11 @@
         dma((Y, CH)),
         dma((Y, CH)),
         dma((TP, CH)),
+        dma((Y,)),
+        dma((1,)),
+        dma((1,)),
+        dma((2,)),
+        dma((2,)),
     ]
     return pl.pallas_call(
         functools.partial(kernel, SP, TP, X),
@@ -590,7 +765,7 @@
         compiler_params=pltpu.CompilerParams(
             collective_id=0, has_side_effects=True, vmem_limit_bytes=60 * 1024 * 1024
         ),
-    )(*args[:9], rate.reshape(1, -1), decay_extra, forget, out_lru, out_fox)
+    )(*args[:9], rate.reshape(1, -1), decay_extra, forget.T, out_lru, out_fox)
 
 
 def columns_of(mesh):

time: 87.9 us -> 70.1 us (0.80)
  Pallas kernels: 84.2 us -> 68 us
  local copies, waits for them, and re-layouts: 3.41 us -> 1.87 us
    pallas_call x1, Pallas kernels: 84.2 us -> 68 us  [shards(): pl.pallas_call(functools.partial(kernel, SP, TP, X), out_shape=jax.ShapeD...]
    unnamed x2 -> x1, local copies, waits for them, and re-layouts: 3.41 us -> 1.87 us
where the time goes in v2:
time: 70.1 us; the launch traced here: 69.9 us
  Pallas kernels  68 us (97%)
  local copies, waits for them, and re-layouts  1.87 us (3%)
    pallas_call x1, Pallas kernels, shards(): pl.pallas_call(functools.partial(kernel, SP, TP, X), out_shape=jax.ShapeD...  68 us
    unnamed x1, local copies, waits for them, and re-layouts  1.87 us

profile of v2, /device:TPU:25, one launch (start us, length us, event | category | flops | bytes accessed | tf_op | source)
XLA Modules:
  0.0 69.9 jit_solution(8413337083107732366)
XLA Ops:
  0.0 68.0 %shard_map.136 = bf16[512,512]{1,0:T(8,128)(2,1)} custom-call(bf16[512,512]{1,0:T(8,128)(2,1)} %tokens.1, bf16[2048,256]{1,0:T(8,128)(2,1)} %lru_in.1, bf16[2048,256]{1,0:T(8,128)(2,1)} %gate_in.1, bf16[2048,256]{1,0:T(8,128)(2,1)} %query_w.1, bf16[2048,256]{1,0:T(8,128)(2,1)} %key_w.1, bf16[2048,256]{1,0:T(8,128)(2,1)} %value_w.1, bf16[4,1024]{1,0:T(4,128)(2,1)} %conv_w.1, ...), custom_call_target="tpu_custom_call" | custom-call | tf_op jit(solution)/shard_map/pallas_call | solution.py:759
  68.0 1.9 %copy.16 = bf16[512,512]{1,0:T(8,128)(2,1)} copy(bf16[512,512]{1,0:T(8,128)(2,1)} %shard_map.136) | data formatting | bytes 1048576

commit v3 on v2

--- a/solution.py
+++ b/solution.py
@@ -373,7 +373,7 @@
             end_copy(k).start()
 
     score_scale = HEAD_DIM ** (-0.5)
-    qc = rc
+    qc = rows // 2
 
     def attend(j, diagonal, far_first=None):
         other = far_first is not None
@@ -689,7 +689,7 @@
     H = fw // HEAD_DIM
     Y = TP // 2
     Z = SP // X
-    CH = 2
+    CH = 4
     vm = pl.BlockSpec(memory_space=pltpu.VMEM)
     hbm = pl.BlockSpec(memory_space=pl.ANY)
     dma = pltpu.SemaphoreType.DMA

time: 70.1 us -> 68.7 us (0.980)
  Pallas kernels: 68 us -> 66.6 us
    pallas_call x1, Pallas kernels: 68 us -> 66.6 us  [shards(): pl.pallas_call(functools.partial(kernel, SP, TP, X), out_shape=jax.ShapeD...]
where the time goes in v3:
time: 68.7 us; the launch traced here: 68.5 us
  Pallas kernels  66.6 us (97%)
  local copies, waits for them, and re-layouts  1.87 us (3%)
    pallas_call x1, Pallas kernels, shards(): pl.pallas_call(functools.partial(kernel, SP, TP, X), out_shape=jax.ShapeD...  66.6 us
    unnamed x1, local copies, waits for them, and re-layouts  1.87 us

profile of v3, /device:TPU:25, one launch (start us, length us, event | category | flops | bytes accessed | tf_op | source)
XLA Modules:
  0.0 68.5 jit_solution(11853661333184795605)
XLA Ops:
  0.0 66.6 %shard_map.136 = bf16[512,512]{1,0:T(8,128)(2,1)} custom-call(bf16[512,512]{1,0:T(8,128)(2,1)} %tokens.1, bf16[2048,256]{1,0:T(8,128)(2,1)} %lru_in.1, bf16[2048,256]{1,0:T(8,128)(2,1)} %gate_in.1, bf16[2048,256]{1,0:T(8,128)(2,1)} %query_w.1, bf16[2048,256]{1,0:T(8,128)(2,1)} %key_w.1, bf16[2048,256]{1,0:T(8,128)(2,1)} %value_w.1, bf16[4,1024]{1,0:T(4,128)(2,1)} %conv_w.1, ...), custom_call_target="tpu_custom_call" | custom-call | tf_op jit(solution)/shard_map/pallas_call | solution.py:759
  66.6 1.9 %copy.16 = bf16[512,512]{1,0:T(8,128)(2,1)} copy(bf16[512,512]{1,0:T(8,128)(2,1)} %shard_map.136) | data formatting | bytes 1048576
